TPU v7x, 32 devices: a whole 2x2x4 slice. The times are simulated.
32 devices in a mesh: ra: 8 (over z, y), cb: 4 (over x, core).
Axes of the slice: x: 2, y: 2, z: 4, core: 2. Of those that a mesh axis runs over, the one named last changes fastest.
Arguments:
- tokens: bfloat16 [512, 4096], P(None, 'cb'), may hold values from -82 to 82
- gate_weight: float32 [2, 4096, 11264], P(None, 'cb', 'ra'), may hold values from -0.09375 to 0.09375
- up_weight: float32 [2, 4096, 11264], P(None, 'cb', 'ra'), may hold values from -0.09375 to 0.09375
- down_weight: float32 [2, 11264, 4096], P(None, 'ra', 'cb'), may hold values from -0.0546875 to 0.0546875
- gate_scale: float32 [2, 11264], P(None, 'ra'), may hold values from 0.5 to 2
- up_scale: float32 [2, 11264], P(None, 'ra'), may hold values from 0.5 to 2
- down_scale: float32 [2, 4096], P(None, 'cb'), may hold values from 0.5 to 2
- norm_gain: float32 [2, 4096], P(None, 'cb'), may hold values from 0.1 to 1.9
- conv_taps: float32 [2, 3, 11264], P(None, None, 'ra'), may hold values from -3 to 3
- conv_bias: float32 [2, 11264], P(None, 'ra'), may hold values from -3 to 3
Outputs:
- layer_out: bfloat16 [512, 4096], P(None, 'cb')
All inputs are finite; a program needn't handle non-finite values.
Results may differ from a plain program's by a relative error of at most 0.012.
Values may be sent and summed in bfloat16 or wider, within the bound.
A program may use at most 128 MiB of HBM per device.

v0:
```python
import jax
import jax.numpy as jnp
from jax import lax
from jax.sharding import PartitionSpec as P

D = 4096
LAYERS = 2
norm_eps = 1e-06
residual_scale = 0.25


def activate(gate, upward, taps, bias):
    padded = jnp.pad(gate, ((1, 1), (0, 0)))
    mixed = taps[0] * padded[:-2] + taps[1] * padded[1:-1] + taps[2] * padded[2:] + bias
    return (jax.nn.silu(mixed) * upward).astype(jnp.bfloat16)


def per_device(
    tokens,
    gate_weight,
    up_weight,
    down_weight,
    gate_scale,
    up_scale,
    down_scale,
    norm_gain,
    conv_taps,
    conv_bias,
):
    hstate = tokens
    for layer in range(LAYERS):
        wide = hstate.astype(jnp.float32)
        squares_part = jnp.sum(wide * wide, axis=1)
        operand = (wide * norm_gain[layer]).astype(jnp.bfloat16)
        gate_part = jnp.dot(
            operand, gate_weight[layer].astype(jnp.bfloat16), preferred_element_type=jnp.float32
        )
        up_part = jnp.dot(
            operand, up_weight[layer].astype(jnp.bfloat16), preferred_element_type=jnp.float32
        )
        gate_sum, up_sum, square_sum = lax.psum((gate_part, up_part, squares_part), "cb")
        rscale = lax.rsqrt(square_sum / D + norm_eps)[:, None]
        gate = gate_sum * rscale * gate_scale[layer]
        upward = up_sum * rscale * up_scale[layer]
        hidden = activate(gate, upward, conv_taps[layer], conv_bias[layer])
        term = jnp.dot(
            hidden, down_weight[layer].astype(jnp.bfloat16), preferred_element_type=jnp.float32
        )
        branch = lax.psum(term, "ra") * down_scale[layer]
        hstate = (residual_scale * wide + branch).astype(jnp.bfloat16)
    return hstate


def solution(mesh):
    in_specs = (
        P(None, "cb"),
        P(None, "cb", "ra"),
        P(None, "cb", "ra"),
        P(None, "ra", "cb"),
        P(None, "ra"),
        P(None, "ra"),
        P(None, "cb"),
        P(None, "cb"),
        P(None, None, "ra"),
        P(None, "ra"),
    )
    out_specs = P(None, "cb")
    return jax.shard_map(
        per_device, mesh=mesh, in_specs=in_specs, out_specs=out_specs, check_vma=False
    )
```

profile of v0, /device:TPU:0, one launch (start us, length us, event | category | flops | bytes accessed | tf_op | source)
XLA Modules:
  0.0 497.1 jit_solution(6274130120586286872)
XLA Ops:
  6.5 0.8 fusion.24
  7.3 4.9 convert.13
  12.2 9.4 %convert.12 = bf16[2,1024,1408]{2,1,0:T(8,128)(2,1)} convert(f32[2,1024,1408]{2,1,0:T(8,128)} %param.11) | non-fusion elementwise | flops 2883584 | bytes 17301504 | tf_op jit(solution)/shard_map/convert.5
  21.6 3.4 fusion.4
  25.1 3.4 fusion.5
  28.4 0.0 all-reduce.15.cloned.1.call-update
  28.5 0.0 all-reduce.9.cloned.1.call-start
  28.5 7.7 %convert.14 = bf16[2,1408,1024]{2,1,0:T(8,128)(2,1)} convert(f32[2,1408,1024]{2,1,0:T(8,128)} %param.13) | non-fusion elementwise | flops 2883584 | bytes 17301504 | tf_op jit(solution)/shard_map/convert.3
  36.2 0.3 fusion.9
  36.5 9.1 %psum.57 = f32[512]{0:T(512)S(1)} all-reduce(f32[512]{0:T(512)S(1)} %fusion.9), channel_id=1, replica_groups=mesh['ra'=8,'cb'=4] {'cb'}, use_global_device_ids=true, to_apply=%region_2.0 | all-reduce | flops 512 | bytes 4096 | tf_op jit(solution)/shard_map/psum | solution.py:41
  45.7 0.1 slice_reduce_fusion
  45.7 0.1 slice_reduce_fusion.5
  45.8 96.7 %all-reduce.15.cloned.1.call-done = (f32[512,1408]{1,0:T(8,128)}, f32[512,1408]{1,0:T(8,128)}) async-done(((f32[512,1408]{1,0:T(8,128)}, f32[512,1408]{1,0:T(8,128)}), (f32[512,1408]{1,0:T(8,128)}, f32[512,1408]{1,0:T(8,128)})) %all-reduce.15.cloned.1.call-update) | async-done | bytes 5767184 | tf_op jit(solution)/shard_map/psum | solution.py:41
  142.5 2.3 multiply_multiply_fusion.1
  144.8 1.2 copy-done
  146.0 6.1 %fusion.3 = f32[512,1024]{1,0:T(8,128)} fusion(bf16[2,1408,1024]{2,1,0:T(8,128)(2,1)S(1)} %copy-done, f32[512,1408]{1,0:T(8,128)} %get-tuple-element.19, f32[512,1408]{1,0:T(8,128)S(1)} %multiply_multiply_fusion.1, f32[1408]{0:T(1024)S(1)} %get-tuple-element.14, f32[1408]{0:T(1024)S(1)} %get-tuple-element.27, f32[1408]{0:T(1024)S(1)} %get-tuple-element.6, ...), kind=kOutput, calls=%fused_computation.13 | convolution fusion | flops 1486487552 | bytes 10790912 | tf_op jit(solution)/shard_map/dot_general | solution.py:46
  152.1 0.0 all-reduce.9.cloned.1.call-update
  152.1 0.0 all-reduce.13.cloned.1.call-start
  152.2 102.5 %all-reduce.9.cloned.1.call-done = f32[512,1024]{1,0:T(8,128)} async-done(((f32[512,1024]{1,0:T(8,128)}), f32[512,1024]{1,0:T(8,128)}) %all-reduce.9.cloned.1.call-update) | async-done | bytes 2097168 | tf_op jit(solution)/shard_map/psum | solution.py:49
  254.7 2.3 fusion.13
  257.0 5.3 %fusion.2 = f32[512,1408]{1,0:T(8,128)} fusion(bf16[2,1024,1408]{2,1,0:T(8,128)(2,1)} %convert.12, bf16[512,1024]{1,0:T(8,128)(2,1)S(1)} %get-tuple-element.22, f32[1024]{0:T(1024)S(1)} %bitcast.26), kind=kOutput, calls=%fused_computation.11 | convolution fusion | flops 1477967872 | bytes 6819840 | tf_op jit(solution)/shard_map/dot_general | solution.py:35
  262.3 3.5 fusion.1
  265.8 0.0 all-reduce.13.cloned.1.call-update
  265.8 0.0 all-reduce.11.cloned.1.call-start
  265.8 6.3 %psum.61 = f32[512]{0:T(512)S(1)} all-reduce(f32[512]{0:T(512)S(1)} %get-tuple-element.21), channel_id=1, replica_groups=mesh['ra'=8,'cb'=4] {'cb'}, use_global_device_ids=true, to_apply=%region_7.8 | all-reduce | flops 512 | bytes 4096 | tf_op jit(solution)/shard_map/psum | solution.py:41
  272.2 104.1 %all-reduce.13.cloned.1.call-done = (f32[512,1408]{1,0:T(8,128)}, f32[512,1408]{1,0:T(8,128)}) async-done(((f32[512,1408]{1,0:T(8,128)}, f32[512,1408]{1,0:T(8,128)}), (f32[512,1408]{1,0:T(8,128)}, f32[512,1408]{1,0:T(8,128)})) %all-reduce.13.cloned.1.call-update) | async-done | bytes 5767184 | tf_op jit(solution)/shard_map/psum | solution.py:41
  376.3 2.3 multiply_multiply_fusion
  378.6 0.4 copy-done.9
  379.0 6.0 %fusion = f32[512,1024]{1,0:T(8,128)} fusion(bf16[2,1408,1024]{2,1,0:T(8,128)(2,1)} %convert.14, f32[512,1408]{1,0:T(8,128)S(1)} %copy-done.9, f32[512,1408]{1,0:T(8,128)S(1)} %multiply_multiply_fusion, f32[1408]{0:T(1024)S(1)} %get-tuple-element.13, f32[1408]{0:T(1024)S(1)} %get-tuple-element.28, f32[1408]{0:T(1024)S(1)} %get-tuple-element.9, ...), kind=kOutput, calls=%fused_computation.7 | convolution fusion | flops 1486487552 | bytes 10778112 | tf_op jit(solution)/shard_map/dot_general | solution.py:46
  385.0 0.0 all-reduce.11.cloned.1.call-update
  385.0 102.6 %all-reduce.11.cloned.1.call-done = f32[512,1024]{1,0:T(8,128)} async-done(((f32[512,1024]{1,0:T(8,128)}), f32[512,1024]{1,0:T(8,128)}) %all-reduce.11.cloned.1.call-update) | async-done | bytes 2097168 | tf_op jit(solution)/shard_map/psum | solution.py:49
  487.6 2.9 fusion.11
  (28 shorter events, 0.1 us)
Async XLA Ops:
  6.5 136.0 %all-reduce.15.cloned.1.call-start = ((), (), s32[]{:S(2)}) async-start(), calls=%async_computation.3 | async-start | bytes 11534336 | tf_op jit(solution)/shard_map/psum | solution.py:41
  12.2 9.4 %copy-start.1 = (bf16[2,1024,1408]{2,1,0:T(8,128)(2,1)}, bf16[2,1024,1408]{2,1,0:T(8,128)(2,1)S(1)}, u32[]{:S(2)}) copy-start(bf16[2,1024,1408]{2,1,0:T(8,128)(2,1)S(1)} %convert.13) | copy-start | bytes 17301508
  12.2 9.4 %copy-start.3 = (bf16[512,1024]{1,0:T(8,128)(2,1)S(1)}, bf16[512,1024]{1,0:T(8,128)(2,1)}, u32[]{:S(2)}) copy-start(bf16[512,1024]{1,0:T(8,128)(2,1)} %param.10) | copy-start | bytes 3145732
  21.6 3.4 copy-start.2
  28.4 17.2 %copy-start.5 = (f32[2,1408]{1,0:T(2,128)S(1)}, f32[2,1408]{1,0:T(2,128)}, u32[]{:S(2)}) copy-start(f32[2,1408]{1,0:T(2,128)} %param.14) | copy-start | bytes 33796
  28.4 17.2 %copy-start.6 = (f32[2,1408]{1,0:T(2,128)S(1)}, f32[2,1408]{1,0:T(2,128)}, u32[]{:S(2)}) copy-start(f32[2,1408]{1,0:T(2,128)} %param.15) | copy-start | bytes 33796
  28.5 17.2 %copy-start.7 = (f32[2,1408]{1,0:T(2,128)S(1)}, f32[2,1408]{1,0:T(2,128)}, u32[]{:S(2)}) copy-start(f32[2,1408]{1,0:T(2,128)} %param.19) | copy-start | bytes 33796
  28.5 17.3 %copy-start.4 = (f32[2,3,1408]{2,0,1:T(2,128)S(1)}, f32[2,3,1408]{2,0,1:T(2,128)}, u32[]{:S(2)}) copy-start(f32[2,3,1408]{2,0,1:T(2,128)} %param.18) | copy-start | bytes 101380
  28.5 226.3 %all-reduce.9.cloned.1.call-start = ((), (), s32[]{:S(2)}) async-start(), calls=%async_computation | async-start | bytes 4194304 | tf_op jit(solution)/shard_map/psum | solution.py:49
  142.5 3.5 copy-start
  146.0 6.1 %copy-start.8 = (f32[2,1024]{1,0:T(2,128)S(1)}, f32[2,1024]{1,0:T(2,128)}, u32[]{:S(2)}) copy-start(f32[2,1024]{1,0:T(2,128)} %param.16) | copy-start | bytes 24580
  152.1 224.2 %all-reduce.13.cloned.1.call-start = ((), (), s32[]{:S(2)}) async-start(), calls=%async_computation.2 | async-start | bytes 11534336 | tf_op jit(solution)/shard_map/psum | solution.py:41
  254.7 7.6 %slice-start = ((s8[5767168]{0:T(1024)(128)(4,1)}), s8[4194304]{0:T(1024)(128)(4,1)S(1)}, s32[]{:S(2)}) async-start(s8[5767168]{0:T(1024)(128)(4,1)} %bitcast.22), calls=%async_computation.4 | async-start | bytes 8388608
  257.0 5.3 %slice-start.1 = ((s8[5767168]{0:T(1024)(128)(4,1)}), s8[1572864]{0:T(1024)(128)(4,1)S(1)}, s32[]{:S(2)}) async-start(s8[5767168]{0:T(1024)(128)(4,1)} %bitcast.22), calls=%async_computation.5 | async-start | bytes 3145728
  265.8 221.8 %all-reduce.11.cloned.1.call-start = ((), (), s32[]{:S(2)}) async-start(), calls=%async_computation.1 | async-start | bytes 4194304 | tf_op jit(solution)/shard_map/psum | solution.py:49
  376.3 2.7 copy-start.9
Sparse Core Ops, SparseCore 0:
  28.6 113.9 all-reduce.14
  152.2 102.4 all-reduce.8
  265.9 110.3 all-reduce.12
  385.1 102.4 all-reduce.10
where the time goes:
time: 497 us
  waiting for transfers between devices  406 us (82%)
  other arithmetic  31.9 us (6%)
  matrix products  27.6 us (6%)
  blocking collectives  15.4 us (3%)
  between operations  13.3 us (3%)
    psum x2, waiting for transfers between devices, per_device(): branch = lax.psum(term, 'ra') * down_scale[layer]  205 us
    psum x2, waiting for transfers between devices, per_device(): lax.psum((gate_part, up_part, squares_part), 'cb')  201 us
    another operation x3, other arithmetic  21.9 us
    psum x2, blocking collectives, per_device(): lax.psum((gate_part, up_part, squares_part), 'cb')  15.4 us
    dot_general x2, matrix products, per_device(): jnp.dot(hidden, down_weight[layer].astype(jnp.bfloat16), preferred_elemen...  12 us
  transfers between devices with their start and end apart: 4, of which 4 were waited for; matrix products, arithmetic and copies ran while one was open for 2% of the time, Pallas kernels for 0%

commit v1 on v0

--- a/solution.py
+++ b/solution.py
@@ -46,7 +46,7 @@
         term = jnp.dot(
             hidden, down_weight[layer].astype(jnp.bfloat16), preferred_element_type=jnp.float32
         )
-        branch = lax.psum(term, "ra") * down_scale[layer]
+        branch = jnp.sum(lax.all_gather(term, "ra"), axis=0) * down_scale[layer]
         hstate = (residual_scale * wide + branch).astype(jnp.bfloat16)
     return hstate
 

time: 497 us -> 760 us (1.53)
  waiting for transfers between devices: 406 us -> 655 us
  other arithmetic: 31.9 us -> 45.9 us
    all_gather x0 -> x2, waiting for transfers between devices: none -> 455 us  [per_device(): branch = jnp.sum(lax.all_gather(term, 'ra'), axis=0) * down_scale[layer]]
    psum x2 -> x0, waiting for transfers between devices: 205 us -> none  [per_device(): branch = lax.psum(term, 'ra') * down_scale[layer]]
    reduce_sum x0 -> x2, other arithmetic: none -> 15.9 us  [per_device(): branch = jnp.sum(lax.all_gather(term, 'ra'), axis=0) * down_scale[layer]]
  transfers between devices with their start and end apart: 4 -> 4, of which waited for: 4 -> 4; matrix products, arithmetic and copies ran while one was open for 2% -> 1% of each run, Pallas kernels for 0% -> 0%
where the time goes in v1:
time: 760 us
  waiting for transfers between devices  655 us (86%)
  other arithmetic  45.9 us (6%)
  matrix products  27.6 us (4%)
  blocking collectives  15 us (2%)
  between operations  13.3 us (2%)
    all_gather x2, waiting for transfers between devices, per_device(): branch = jnp.sum(lax.all_gather(term, 'ra'), axis=0) * down_scale[layer]  455 us
    psum x2, waiting for transfers between devices, per_device(): lax.psum((gate_part, up_part, squares_part), 'cb')  200 us
    another operation x3, other arithmetic  21.9 us
    reduce_sum x2, other arithmetic, per_device(): branch = jnp.sum(lax.all_gather(term, 'ra'), axis=0) * down_scale[layer]  15.9 us
  transfers between devices with their start and end apart: 4, of which 4 were waited for; matrix products, arithmetic and copies ran while one was open for 1% of the time, Pallas kernels for 0%

profile of v1, /device:TPU:0, one launch (start us, length us, event | category | flops | bytes accessed | tf_op | source)
XLA Modules:
  0.0 760.0 jit_solution(11928785026625512524)
XLA Ops:
  6.5 0.8 fusion.24
  7.3 4.9 convert.13
  12.2 9.4 %convert.12 = bf16[2,1024,1408]{2,1,0:T(8,128)(2,1)} convert(f32[2,1024,1408]{2,1,0:T(8,128)} %param.11) | non-fusion elementwise | flops 2883584 | bytes 17301504 | tf_op jit(solution)/shard_map/convert.5
  21.6 3.4 fusion.4
  25.0 3.5 fusion.5
  28.5 0.0 all-reduce.9.cloned.1.call-update
  28.5 0.0 all-gather.5.cloned.1.call-start
  28.6 7.7 %convert.14 = bf16[2,1408,1024]{2,1,0:T(8,128)(2,1)} convert(f32[2,1408,1024]{2,1,0:T(8,128)} %param.13) | non-fusion elementwise | flops 2883584 | bytes 17301504 | tf_op jit(solution)/shard_map/convert.3
  36.3 0.3 fusion.9
  36.5 9.1 %psum.43 = f32[512]{0:T(512)S(1)} all-reduce(f32[512]{0:T(512)S(1)} %fusion.9), channel_id=1, replica_groups=mesh['ra'=8,'cb'=4] {'cb'}, use_global_device_ids=true, to_apply=%region_2.0 | all-reduce | flops 512 | bytes 4096 | tf_op jit(solution)/shard_map/psum | solution.py:41
  45.7 0.1 slice_reduce_fusion
  45.8 0.1 slice_reduce_fusion.5
  45.9 96.7 %all-reduce.9.cloned.1.call-done = (f32[512,1408]{1,0:T(8,128)}, f32[512,1408]{1,0:T(8,128)}) async-done(((f32[512,1408]{1,0:T(8,128)}, f32[512,1408]{1,0:T(8,128)}), (f32[512,1408]{1,0:T(8,128)}, f32[512,1408]{1,0:T(8,128)})) %all-reduce.9.cloned.1.call-update) | async-done | bytes 5767184 | tf_op jit(solution)/shard_map/psum | solution.py:41
  142.6 2.3 multiply_multiply_fusion.1
  144.8 1.2 copy-done
  146.1 6.0 fusion.3
  152.1 0.2 all-reduce.7.cloned.1.call-start
  152.3 227.4 %all-gather.5.cloned.1.call-done = f32[4096,1024]{1,0:T(8,128)} async-done(((f32[512,1024]{1,0:T(8,128)}), f32[4096,1024]{1,0:T(8,128)}) %all-gather.5.cloned.1.call-update) | async-done | bytes 16777232 | tf_op jit(solution)/shard_map/all_gather | solution.py:49
  379.7 8.0 %reduce_sum.37 = f32[512,1024]{1,0:T(8,128)S(1)} reduce(f32[8,512,1024]{2,1,0:T(8,128)} %bitcast.24, f32[]{:T(128)} %constant.12.clone.1), dimensions={0}, to_apply=%region_4.5 | reduce | flops 3670016 | bytes 18874372 | tf_op jit(solution)/shard_map/reduce_sum | solution.py:49
  387.7 1.9 fusion.13
  389.6 5.3 fusion.2
  394.9 3.5 fusion.1
  398.4 0.0 all-reduce.7.cloned.1.call-update
  398.4 0.0 all-gather.7.cloned.1.call-start
  398.5 5.9 psum.46
  404.3 103.5 %all-reduce.7.cloned.1.call-done = (f32[512,1408]{1,0:T(8,128)}, f32[512,1408]{1,0:T(8,128)}) async-done(((f32[512,1408]{1,0:T(8,128)}, f32[512,1408]{1,0:T(8,128)}), (f32[512,1408]{1,0:T(8,128)}, f32[512,1408]{1,0:T(8,128)})) %all-reduce.7.cloned.1.call-update) | async-done | bytes 5767184 | tf_op jit(solution)/shard_map/psum | solution.py:41
  507.8 2.3 multiply_multiply_fusion
  510.1 0.4 copy-done.9
  510.5 6.0 fusion
  516.5 227.6 %all-gather.7.cloned.1.call-done = f32[4096,1024]{1,0:T(8,128)} async-done(((f32[512,1024]{1,0:T(8,128)}), f32[4096,1024]{1,0:T(8,128)}) %all-gather.7.cloned.1.call-update) | async-done | bytes 16777232 | tf_op jit(solution)/shard_map/all_gather | solution.py:49
  744.1 8.0 %reduce_sum.39 = f32[512,1024]{1,0:T(8,128)S(1)} reduce(f32[8,512,1024]{2,1,0:T(8,128)} %bitcast.25, f32[]{:T(128)} %constant.12.clone.1), dimensions={0}, to_apply=%region_9.10 | reduce | flops 3670016 | bytes 18874372 | tf_op jit(solution)/shard_map/reduce_sum | solution.py:49
  752.1 1.3 fusion.11
  (30 shorter events, 0.1 us)
Async XLA Ops:
  6.5 136.0 %all-reduce.9.cloned.1.call-start = ((), (), s32[]{:S(2)}) async-start(), calls=%async_computation.3 | async-start | bytes 11534336 | tf_op jit(solution)/shard_map/psum | solution.py:41
  12.2 9.4 %copy-start.1 = (bf16[2,1024,1408]{2,1,0:T(8,128)(2,1)}, bf16[2,1024,1408]{2,1,0:T(8,128)(2,1)S(1)}, u32[]{:S(2)}) copy-start(bf16[2,1024,1408]{2,1,0:T(8,128)(2,1)S(1)} %convert.13) | copy-start | bytes 17301508
  12.2 9.4 %copy-start.3 = (bf16[512,1024]{1,0:T(8,128)(2,1)S(1)}, bf16[512,1024]{1,0:T(8,128)(2,1)}, u32[]{:S(2)}) copy-start(bf16[512,1024]{1,0:T(8,128)(2,1)} %param.10) | copy-start | bytes 3145732
  21.6 3.4 copy-start.2
  28.5 17.2 %copy-start.5 = (f32[2,1408]{1,0:T(2,128)S(1)}, f32[2,1408]{1,0:T(2,128)}, u32[]{:S(2)}) copy-start(f32[2,1408]{1,0:T(2,128)} %param.14) | copy-start | bytes 33796
  28.5 17.2 %copy-start.6 = (f32[2,1408]{1,0:T(2,128)S(1)}, f32[2,1408]{1,0:T(2,128)}, u32[]{:S(2)}) copy-start(f32[2,1408]{1,0:T(2,128)} %param.15) | copy-start | bytes 33796
  28.5 17.2 %copy-start.7 = (f32[2,1408]{1,0:T(2,128)S(1)}, f32[2,1408]{1,0:T(2,128)}, u32[]{:S(2)}) copy-start(f32[2,1408]{1,0:T(2,128)} %param.19) | copy-start | bytes 33796
  28.5 17.3 %copy-start.4 = (f32[2,3,1408]{2,0,1:T(2,128)S(1)}, f32[2,3,1408]{2,0,1:T(2,128)}, u32[]{:S(2)}) copy-start(f32[2,3,1408]{2,0,1:T(2,128)} %param.18) | copy-start | bytes 101380
  28.5 351.2 %all-gather.5.cloned.1.call-start = ((), (), s32[]{:S(2)}) async-start(), calls=%async_computation | async-start | bytes 18874368 | tf_op jit(solution)/shard_map/all_gather | solution.py:49
  142.6 3.5 copy-start
  146.1 6.2 copy-start.8
  152.1 355.7 %all-reduce.7.cloned.1.call-start = ((), (), s32[]{:S(2)}) async-start(), calls=%async_computation.2 | async-start | bytes 11534336 | tf_op jit(solution)/shard_map/psum | solution.py:41
  387.7 7.2 slice-start
  389.6 5.3 slice-start.1
  398.4 345.7 %all-gather.7.cloned.1.call-start = ((), (), s32[]{:S(2)}) async-start(), calls=%async_computation.1 | async-start | bytes 18874368 | tf_op jit(solution)/shard_map/all_gather | solution.py:49
  507.8 2.7 copy-start.9
Sparse Core Ops, SparseCore 0:
  28.6 113.9 all-reduce.8
  152.2 227.4 all-gather.4
  398.5 109.2 all-reduce.6
  516.6 227.4 all-gather.6
